TPU v7x, 32 devices: a whole 2x2x4 slice. The times are simulated.
32 devices in a mesh: sp: 8 (over z, y), tp: 4 (over x, core).
Axes of the slice: x: 2, y: 2, z: 4, core: 2. Of those that a mesh axis runs over, the one named last changes fastest.
Arguments:
- tokens: bfloat16 [3072, 2048], P(('sp', 'tp')), may hold values from -8 to 8, as said below
- query_weight: bfloat16 [2048, 1024], P(None, 'tp'), as said below
- key_weight: bfloat16 [2048, 256], P(None, 'tp'), as said below
- value_weight: bfloat16 [2048, 256], P(None, 'tp'), may hold values from -0.125 to 0.125
- out_weight: bfloat16 [1024, 2048], P('tp'), may hold values from -0.75 to 0.75
- query_gain: bfloat16 [16, 64], P('tp'), may hold values from 0.5 to 6.5
- key_gain: bfloat16 [4, 64], P('tp'), may hold values from 0.5 to 6.5
Outputs:
- mixed: bfloat16 [3072, 2048], P(('sp', 'tp'))
- log_sums: float32 [16, 3072], P('tp', 'sp')
Inputs may be any that keep to these rules, and one draw needn't show every extreme that they name: Each block of 384 consecutive tokens has a mean vector of its own. `query_weight`: entries are those of a weight over 2048 inputs, of magnitude at most 6 / sqrt(2048). `key_weight`: entries are those of a weight over 2048 inputs, of magnitude at most 6 / sqrt(2048).
All inputs are finite; a program needn't handle non-finite values.
Results may differ from a plain program's by a relative error of at most 0.028.
Values may be sent and summed in bfloat16 or wider, within the bound.
A program may use at most 64 MiB of HBM per device.

v0:
```python
import functools
import math

import jax
import jax.numpy as jnp
from jax import lax
from jax.experimental import pallas as pl
from jax.experimental.pallas import tpu as pltpu
from jax.sharding import PartitionSpec as P

GRID_W = 64
ROPE_BASE = 10000.0
EPS = 1e-06
LOG2E = math.log2(math.e)
LN2 = math.log(2.0)
ONES = 16
MESH = pl.DeviceIdType.MESH
F32 = jnp.float32
BF16 = jnp.bfloat16


def prepare(x, gain, tables):
    quarter = x.shape[0] // 4
    x = x * lax.rsqrt(jnp.mean(x * x, axis=0, keepdims=True) + EPS) * gain
    a, b, c, d = (x[i * quarter : (i + 1) * quarter] for i in range(4))
    row_cos, row_sin, col_cos, col_sin = tables
    return jnp.concatenate(
        [
            a * row_cos - b * row_sin,
            b * row_cos + a * row_sin,
            c * col_cos - d * col_sin,
            d * col_cos + c * col_sin,
        ],
        axis=0,
    )


def angle_tables(first, count, quarter):
    place = first + lax.broadcasted_iota(jnp.int32, (quarter, count), 1)
    order = lax.broadcasted_iota(jnp.int32, (quarter, count), 0).astype(F32)
    freq = jnp.exp(order * (-math.log(ROPE_BASE) / quarter))
    shift = GRID_W.bit_length() - 1
    row = lax.shift_right_logical(place, shift).astype(F32) * freq
    col = jnp.bitwise_and(place, GRID_W - 1).astype(F32) * freq
    return (jnp.cos(row), jnp.sin(row), jnp.cos(col), jnp.sin(col))


def kernel(
    n_sp,
    n_tp,
    chunks,
    tok_hbm,
    wq_hbm,
    wk_hbm,
    wv_hbm,
    wo_hbm,
    qg_ref,
    kg_ref,
    mixed_ref,
    log_ref,
    tok,
    wq,
    wkv,
    wo,
    gains,
    raw,
    queries,
    kv,
    top,
    acc,
    att_own,
    att_out,
    att_in,
    part_out,
    part_in,
    local_sem,
    tok_send,
    tok_recv,
    wo_send,
    wo_recv,
    kv_send,
    kv_recv,
    att_send,
    att_recv,
    part_send,
    part_recv,
):
    sp = lax.axis_index("sp")
    tp = lax.axis_index("tp")
    pairs = n_tp // 2
    cols = n_sp // 2
    pair, core = tp // 2, tp % 2
    mate = pair * 2 + (1 - core)
    col, side = sp // 2, sp % 2
    other = col * 2 + (1 - side)
    rows = tok.shape[1]
    heads, width = qg_ref.shape
    kv_heads = kg_ref.shape[0]
    share = heads // kv_heads
    count = rows * n_tp

    def across(i):
        return lax.rem(pair + i, pairs) * 2 + core

    kv_cols = wk_hbm.shape[0]
    loads = [
        pltpu.make_async_copy(src, dst, local_sem.at[i])
        for i, (src, dst) in enumerate(
            ((tok_hbm, tok.at[tp]), (wq_hbm, wq), (wk_hbm, wkv.at[0:kv_cols]), (wv_hbm, wkv.at[kv_cols:]), (wo_hbm, wo.at[core]))
        )
    ]
    for load in loads:
        load.start()

    barrier = pltpu.get_barrier_semaphore()
    peers = 0
    for i in range(1, pairs):
        pl.semaphore_signal(barrier, inc=1, device_id={"tp": across(i)}, device_id_type=MESH)
        peers += 1
    pl.semaphore_signal(barrier, inc=1, device_id={"tp": mate}, device_id_type=MESH)
    pl.semaphore_signal(barrier, inc=1, device_id={"sp": other}, device_id_type=MESH)
    peers += 2
    for i in range(1, cols):
        peer = lax.rem(col + i, cols) * 2 + side
        pl.semaphore_signal(barrier, inc=1, device_id={"sp": peer}, device_id_type=MESH)
        peers += 1
    pl.semaphore_wait(barrier, peers)

    def send(src, dst, send_sem, recv_sem, where):
        return pltpu.make_async_remote_copy(
            src_ref=src,
            dst_ref=dst,
            send_sem=send_sem,
            recv_sem=recv_sem,
            device_id=where,
            device_id_type=MESH,
        )

    pending = []

    def go(copy):
        copy.start()
        pending.append(copy)

    def token_copy(block, src, slot, target):
        return send(src, tok.at[block], tok_send.at[slot], tok_recv.at[block], {"tp": target})

    for i in range(1, pairs):
        go(token_copy(tp, tok_hbm, i, across(i)))
    go(token_copy(tp, tok_hbm, 0, mate))

    gains[...] = jnp.zeros_like(gains)
    gains[0:heads, 0:width] = qg_ref[...].astype(F32) * (LOG2E * width ** (-0.5))
    gains[heads : heads + kv_heads, 0:width] = kg_ref[...].astype(F32)
    turned_gains = jnp.transpose(gains[...])
    tables = angle_tables(sp * count, count, width // 4)
    top[...] = jnp.full_like(top, -1e30)
    acc[...] = jnp.zeros_like(acc)
    loads[2].wait()
    loads[3].wait()
    loads[1].wait()
    loads[0].wait()
    query_cols = wq.shape[1]

    def project(block):
        piece = tok[block]
        at = pl.ds(pl.multiple_of(block * rows, rows), rows)
        raw[at, 0:query_cols] = jnp.dot(piece, wq[...], preferred_element_type=F32)
        raw[at, query_cols:] = lax.dot_general(
            piece, wkv[...], (((1,), (1,)), ((), ())), preferred_element_type=F32
        )

    kv_rows = kv_heads * width
    span = 2 * rows

    def span_of(part):
        return pl.ds(pl.multiple_of(part * span, span), span)

    def make_kv(part):
        at = span_of(part)
        turned = jnp.transpose(raw[at, query_cols : query_cols + kv_rows])
        angles = angle_tables(sp * count + part * span, span, width // 4)
        for h in range(kv_heads):
            gain = turned_gains[0:width, heads + h : heads + h + 1]
            keys = prepare(turned[h * width : (h + 1) * width], gain, angles)
            kv[sp, at, h * width : (h + 1) * width] = jnp.transpose(keys).astype(BF16)
        kv[sp, at, kv_rows : 2 * kv_rows] = raw[at, query_cols + kv_rows :].astype(BF16)

    def kv_copy(block, part, slot, where):
        spot = kv.at[block, span_of(part)]
        return send(spot, spot, kv_send.at[slot, part], kv_recv.at[block, part], {"sp": where})

    def near(distance, act):
        for way in (1, -1):
            place = col + distance * way

            @pl.when(jnp.logical_and(place >= 0, place < cols))
            def _():
                act(place)

    def to_column(place, part):
        return kv_copy(sp, part, place, place * 2 + side)

    def to_other(place, part):
        return kv_copy(place * 2 + side, part, cols + place, other)

    def send_kv(part):
        to_other(col, part).start()
        for distance in range(1, cols):
            near(distance, lambda place: to_column(place, part).start())

    def forward(place, part):
        kv_copy(place * 2 + side, part, 0, other).wait_recv()
        to_other(place, part).start()

    project(tp)
    token_copy(mate, tok_hbm, 0, mate).wait_recv()
    project(mate)
    make_kv(pair)
    send_kv(pair)
    for i in range(1, pairs):
        block = across(i)
        token_copy(block, tok_hbm, i, block).wait_recv()
        go(token_copy(block, tok.at[block], pairs + i, mate))
        project(block)
    loads[4].wait()
    wo_copy = send(wo_hbm, wo.at[core], wo_send, wo_recv, {"tp": mate})
    wo_copy.start()
    for i in range(1, pairs):
        block = lax.rem(pair + i, pairs) * 2 + (1 - core)
        token_copy(block, tok_hbm, i, mate).wait_recv()
        project(block)
        part = lax.rem(pair + i, pairs)
        make_kv(part)
        send_kv(part)
    for distance in range(1, cols):
        near(distance, lambda place: forward(place, pair))

    turned = jnp.transpose(raw[:, 0:query_cols])
    for h in range(heads):
        q = prepare(turned[h * width : (h + 1) * width], turned_gains[0:width, h : h + 1], tables)
        queries[h] = q.astype(BF16)

    def attend(block):
        ones = jnp.ones((ONES, count), BF16)
        turned = jnp.transpose(kv[block])
        for g in range(kv_heads):
            keys = kv[block, :, g * width : (g + 1) * width]
            values = turned[kv_rows + g * width : kv_rows + (g + 1) * width]
            values = jnp.concatenate([values, ones], axis=0)
            for h in range(g * share, (g + 1) * share):
                scores = jnp.dot(keys, queries[h], preferred_element_type=F32)
                old = top[h : h + 1, :]
                new = jnp.maximum(old, jnp.max(scores, axis=0, keepdims=True))
                weights = jnp.exp2(scores - new).astype(BF16)
                mixed = jnp.dot(values, weights, preferred_element_type=F32)
                acc[h] = acc[h] * jnp.exp2(old - new) + mixed
                top[h : h + 1, :] = new

    def straight(place):
        for i in range(1, pairs):
            forward(place, lax.rem(pair + i, pairs))
        attend(place * 2 + side)

    def mirrored(place):
        block = place * 2 + (1 - side)
        for part in range(pairs):
            kv_copy(block, part, 0, other).wait_recv()
        attend(block)

    attend(sp)
    mirrored(col)

    def step(distance, carry):
        near(distance, straight)

        @pl.when(distance > 1)
        def _():
            near(distance - 1, mirrored)

        return carry

    lax.fori_loop(1, cols, step, 0)
    near(cols - 1, mirrored)

    finished = []
    for h in range(heads):
        total = acc[h, width : width + 1, :]
        finished.append(acc[h, 0:width, :] / total)
        log_ref[h : h + 1, :] = (top[h : h + 1, :] + jnp.log2(total)) * LN2
    attended = jnp.transpose(jnp.concatenate(finished, axis=0)).astype(BF16)
    for t in range(n_tp):
        piece = attended[t * rows : (t + 1) * rows]

        @pl.when(core == t % 2)
        def _():
            att_own[t // 2] = piece

        @pl.when(core != t % 2)
        def _():
            att_out[t // 2] = piece

    att_copy = send(att_out, att_in, att_send, att_recv, {"tp": mate})
    att_copy.start()
    att_copy.wait_recv()
    wo_copy.wait_recv()
    step_cols = mixed_ref.shape[1] // chunks

    def product(place, n):
        at = slice(n * step_cols, (n + 1) * step_cols)
        return jnp.dot(
            att_own[place], wo[core, :, at], preferred_element_type=F32
        ) + jnp.dot(att_in[place], wo[1 - core, :, at], preferred_element_type=F32)

    def part_copy(i, n):
        slot = (i - 1) * chunks + n
        return send(
            part_out.at[slot],
            part_in.at[slot],
            part_send.at[slot],
            part_recv.at[slot],
            {"tp": across(i)},
        )

    for n in range(chunks):
        for i in range(1, pairs):
            part_out[(i - 1) * chunks + n] = product(lax.rem(pair + i, pairs), n).astype(BF16)
            part_copy(i, n).start()
    for n in range(chunks):
        at = slice(n * step_cols, (n + 1) * step_cols)
        total = product(pair, n)
        for i in range(1, pairs):
            part_copy(i, n).wait_recv()
            total = total + part_in[(i - 1) * chunks + n].astype(F32)
        mixed_ref[:, at] = total.astype(BF16)

    for copy in pending:
        copy.wait_send()
    wo_copy.wait_send()
    att_copy.wait_send()
    for part in range(pairs):
        to_other(col, part).wait_send()
        for distance in range(1, cols):
            near(distance, lambda place: to_column(place, part).wait_send())
            near(distance, lambda place: to_other(place, part).wait_send())
    for n in range(chunks):
        for i in range(1, pairs):
            part_copy(i, n).wait_send()


def body(n_sp, n_tp, tokens, query_weight, key_weight, value_weight, out_weight, query_gain, key_gain):
    rows, depth = tokens.shape
    query_cols = query_weight.shape[1]
    kv_cols = key_weight.shape[1]
    heads, width = query_gain.shape
    kv_heads = key_gain.shape[0]
    group, model = out_weight.shape
    count = rows * n_tp
    pairs, cols = n_tp // 2, n_sp // 2
    chunks = 4
    any_space = pl.BlockSpec(memory_space=pl.ANY)
    vmem = pl.BlockSpec(memory_space=pltpu.VMEM)
    dma = pltpu.SemaphoreType.DMA
    slots = max(pairs - 1, 1) * chunks
    return pl.pallas_call(
        functools.partial(kernel, n_sp, n_tp, chunks),
        out_shape=(
            pltpu.VMEM((rows, model), BF16),
            pltpu.VMEM((heads, count), F32),
        ),
        in_specs=[any_space] * 5 + [vmem] * 2,
        out_specs=(vmem, vmem),
        scratch_shapes=[
            pltpu.VMEM((n_tp, rows, depth), BF16),
            pltpu.VMEM((depth, query_cols), BF16),
            pltpu.VMEM((2 * kv_cols, depth), BF16),
            pltpu.VMEM((2, group, model), BF16),
            pltpu.VMEM((128, 128), F32),
            pltpu.VMEM((count, query_cols + 2 * kv_cols), F32),
            pltpu.VMEM((heads, width, count), BF16),
            pltpu.VMEM((n_sp, count, 2 * kv_heads * width), BF16),
            pltpu.VMEM((heads, count), F32),
            pltpu.VMEM((heads, width + ONES, count), F32),
            pltpu.VMEM((pairs, rows, group), BF16),
            pltpu.VMEM((pairs, rows, group), BF16),
            pltpu.VMEM((pairs, rows, group), BF16),
            pltpu.VMEM((slots, rows, model // chunks), BF16),
            pltpu.VMEM((slots, rows, model // chunks), BF16),
            dma((5,)),
            dma((2 * pairs,)),
            dma((n_tp,)),
            dma,
            dma,
            dma((2 * cols, pairs)),
            dma((n_sp, pairs)),
            dma,
            dma,
            dma((slots,)),
            dma((slots,)),
        ],
        compiler_params=pltpu.CompilerParams(
            collective_id=0, has_side_effects=True, vmem_limit_bytes=60 * 1024 * 1024
        ),
        name="attention",
    )(tokens, query_weight, key_weight.T, value_weight.T, out_weight, query_gain, key_gain)


def solution(mesh):
    return jax.shard_map(
        functools.partial(body, mesh.shape["sp"], mesh.shape["tp"]),
        mesh=mesh,
        in_specs=(
            P(("sp", "tp"), None),
            P(None, "tp"),
            P(None, "tp"),
            P(None, "tp"),
            P("tp", None),
            P("tp", None),
            P("tp", None),
        ),
        out_specs=(P(("sp", "tp"), None), P("tp", "sp")),
        check_vma=False,
    )
```

profile of v0, /device:TPU:0, one launch (start us, length us, event | category | flops | bytes accessed | tf_op | source)
XLA Modules:
  0.0 46.5 jit_solution(2759891391099343596)
XLA Ops:
  0.6 44.5 %attention.1 = (bf16[96,2048]{1,0:T(8,128)(2,1)S(1)}, f32[4,384]{1,0:T(4,128)S(1)}) custom-call(bf16[96,2048]{1,0:T(8,128)(2,1)} %tok_hbm.1, bf16[2048,256]{1,0:T(8,128)(2,1)} %wq_hbm.1, bf16[64,2048]{1,0:T(8,128)(2,1)} %bitcast.2, bf16[64,2048]{1,0:T(8,128)(2,1)} %bitcast.3, bf16[256,2048]{1,0:T(8,128)(2,1)} %wo_hbm.1, bf16[4,64]{1,0:T(4,128)(2,1)} %qg_ref.1, ...), custom_call_target="tpu_custom_call" | custom-call | tf_op jit(solution)/shard_map/attention/pallas_call | solution.py:365
  45.2 0.7 %copy.11 = bf16[96,2048]{1,0:T(8,128)(2,1)} copy(bf16[96,2048]{1,0:T(8,128)(2,1)S(1)} %get-tuple-element.2) | data formatting | bytes 786432
  45.9 0.6 %copy.12 = f32[4,384]{1,0:T(4,128)} copy(f32[4,384]{1,0:T(4,128)S(1)} %get-tuple-element.3) | data formatting | bytes 12288
where the time goes:
time: 46.7 us; the launch traced here: 46.5 us
  Pallas kernels  44.5 us (95%)
  local copies, waits for them, and re-layouts  1.34 us (3%)
  between operations  0.64 us (1%)
    pallas_call x1, Pallas kernels, body(): pl.pallas_call(functools.partial(kernel, n_sp, n_tp, chunks), out_shape=(...  44.5 us
    unnamed x2, local copies, waits for them, and re-layouts  1.34 us

commit v1 on v0

v1 whole, which is shorter than its diff:
```python
import functools
import math

import jax
import jax.numpy as jnp
from jax import lax
from jax.experimental import pallas as pl
from jax.experimental.pallas import tpu as pltpu
from jax.sharding import PartitionSpec as P

GRID_W = 64
ROPE_BASE = 10000.0
EPS = 1e-06
LOG2E = math.log2(math.e)
LN2 = math.log(2.0)
ONES = 16
TILE = 256
AHEAD = 3
BEHIND = 3
LINES = 4
SUBS = 4
MESH = pl.DeviceIdType.MESH
F32 = jnp.float32
BF16 = jnp.bfloat16


def prepare(x, gain, tables):
    quarter = x.shape[0] // 4
    x = x * lax.rsqrt(jnp.mean(x * x, axis=0, keepdims=True) + EPS) * gain
    a, b, c, d = (x[i * quarter : (i + 1) * quarter] for i in range(4))
    row_cos, row_sin, col_cos, col_sin = tables
    return jnp.concatenate(
        [
            a * row_cos - b * row_sin,
            b * row_cos + a * row_sin,
            c * col_cos - d * col_sin,
            d * col_cos + c * col_sin,
        ],
        axis=0,
    )


def angle_tables(place, quarter):
    order = lax.broadcasted_iota(jnp.int32, (quarter, place.shape[1]), 0).astype(F32)
    freq = jnp.exp(order * (-math.log(ROPE_BASE) / quarter))
    shift = GRID_W.bit_length() - 1
    row = lax.shift_right_logical(place, shift).astype(F32) * freq
    col = jnp.bitwise_and(place, GRID_W - 1).astype(F32) * freq
    return (jnp.cos(row), jnp.sin(row), jnp.cos(col), jnp.sin(col))


def kernel(
    n_sp,
    n_tp,
    sizes,
    tok_hbm,
    wq_hbm,
    wk_hbm,
    wv_hbm,
    wo_hbm,
    qg_hbm,
    kg_hbm,
    mixed_ref,
    log_ref,
    tok,
    wall,
    wkv,
    wo,
    qg,
    kg,
    gains,
    raw,
    tabs,
    tabs_late,
    queries,
    kv_early,
    kv_late,
    top,
    acc,
    att_out,
    att_in,
    res,
    local_sem,
    tok_send,
    tok_recv,
    wo_send,
    wo_recv,
    kv_send,
    kv_recv,
    att_send,
    att_recv,
):
    sp = lax.axis_index("sp")
    tp = lax.axis_index("tp")
    pairs = n_tp // 2
    cols = n_sp // 2
    pair, core = tp // 2, tp % 2
    mate = pair * 2 + (1 - core)
    col, side = sp // 2, sp % 2
    other = col * 2 + (1 - side)

    def near_place(k):
        place, bit = col, 1
        while bit < cols:
            if k & bit:
                place = place + bit * (1 - 2 * ((col // bit) % 2))
            bit *= 2
        return place

    beside = near_place(1) * 2 + side
    rows = tok.shape[2]
    heads, width = qg.shape
    kv_heads = kg.shape[0]
    share = heads // kv_heads
    span = 2 * rows
    count = rows * n_tp
    query_cols = wq_hbm.shape[1]
    kv_cols = wk_hbm.shape[0]
    group = wo.shape[2]
    chunks = len(sizes)
    starts = [sum(sizes[:c]) for c in range(chunks)]
    quarter = width // 4

    def across(i):
        return lax.rem(pair + i, pairs) * 2 + core

    loads = [
        pltpu.make_async_copy(src, dst, local_sem.at[i])
        for i, src, dst in (
            (0, tok_hbm, tok.at[0, core]),
            (1, wk_hbm, wkv.at[0:kv_cols]),
            (1, wv_hbm, wkv.at[kv_cols:]),
            (1, wq_hbm, wall.at[:, 0:query_cols]),
            (2, qg_hbm, qg),
            (3, kg_hbm, kg),
            (4, wo_hbm, wo.at[0, core]),
        )
    ]
    for load in loads:
        load.start()

    barrier = pltpu.get_barrier_semaphore()
    peers = 0
    for i in range(1, n_tp):
        pl.semaphore_signal(barrier, inc=1, device_id={"tp": lax.rem(tp + i, n_tp)}, device_id_type=MESH)
        peers += 1
    pl.semaphore_signal(barrier, inc=1, device_id={"sp": other}, device_id_type=MESH)
    peers += 1
    for i in range(1, cols):
        peer = lax.rem(col + i, cols) * 2 + side
        pl.semaphore_signal(barrier, inc=1, device_id={"sp": peer}, device_id_type=MESH)
        peers += 1
    pl.semaphore_wait(barrier, peers)

    def send(src, dst, send_sem, recv_sem, where):
        return pltpu.make_async_remote_copy(
            src_ref=src,
            dst_ref=dst,
            send_sem=send_sem,
            recv_sem=recv_sem,
            device_id=where,
            device_id_type=MESH,
        )

    def wait_sent(spot, sem):
        send(spot, spot, sem, tok_recv.at[0], {"tp": mate}).wait_send()

    def wait_here(spot, sem):
        send(spot, spot, tok_send.at[0], sem, {"tp": mate}).wait_recv()

    def rows_of(c):
        return slice(starts[c], starts[c] + sizes[c])

    def tok_sem(which, slot, c):
        return tok_recv.at[(slot * 2 + which) * chunks + c]

    def token_over(i, c):
        slot = pairs - i
        return send(
            tok_hbm.at[rows_of(c)],
            tok.at[slot, core, rows_of(c)],
            tok_send.at[2 * i],
            tok_sem(0, slot, c),
            {"tp": across(i)},
        )

    def token_on(slot, c):
        spot = tok.at[slot, core, rows_of(c)]
        return send(spot, spot, tok_send.at[2 * slot + 1], tok_sem(1, slot, c), {"tp": mate})

    for c in range(chunks):
        for i in range(1, pairs):
            token_over(i, c).start()
    send(tok_hbm, tok.at[0, core], tok_send.at[0], tok_recv.at[0], {"tp": mate}).start()

    def tokens_sent():
        for n in range(2 * pairs):
            if n != 1:
                wait_sent(tok.at[0, 0], tok_send.at[n])

    sub_rows = group // (4 * SUBS)
    shares = [(way, h) for h in range(SUBS) for way in (1, 0)]
    sides = (side, col % 2)
    friends = (other, beside)

    def wo_rows(way, whose, h):
        at = (2 * way + whose) * SUBS + h
        return pl.ds(pl.multiple_of(at * sub_rows, sub_rows), sub_rows)

    def wo_sem(slot, own, way, h):
        return wo_recv.at[slot, (own * 2 + way) * SUBS + h]

    def wo_over(i, way, h):
        slot = pairs - i
        at = wo_rows(way, sides[way], h)
        return send(
            wo_hbm.at[at], wo.at[slot, core, at], wo_send.at[i, 0], wo_sem(slot, 0, way, h), {"tp": across(i)}
        )

    def wo_on(slot, way, h):
        spot = wo.at[slot, core, wo_rows(way, sides[way], h)]
        return send(spot, spot, wo_send.at[slot, 1], wo_sem(slot, 1, way, h), {"sp": friends[way]})

    def wo_give(slot, way, whose, h):
        spot = wo.at[slot, core, wo_rows(way, whose, h)]
        return send(spot, spot, wo_send.at[slot, 2], wo_recv.at[slot, 4 * SUBS], {"tp": mate})

    send(wo_hbm, wo.at[0, core], wo_send.at[0, 0], wo_recv.at[0, 0], {"tp": mate}).start()
    for way, h in shares:
        for i in range(1, pairs):
            wo_over(i, way, h).start()

    def wo_pass(start, stop):
        for way, h in shares[start:stop]:
            for slot in range(1, pairs):
                wait_here(wo.at[slot, core, wo_rows(way, sides[way], h)], wo_sem(slot, 0, way, h))
                wo_on(slot, way, h).start()
                wo_give(slot, way, sides[way], h).start()

    def wo_take(start, stop):
        for way, h in shares[start:stop]:
            for slot in range(1, pairs):
                wait_here(wo.at[slot, core, wo_rows(way, 1 - sides[way], h)], wo_sem(slot, 1, way, h))
                wo_give(slot, way, 1 - sides[way], h).start()

    def wo_last():
        for slot in range(1, pairs):
            wait_here(wo.at[slot, 1 - core], wo_recv.at[slot, 4 * SUBS])

    def wo_sent():
        wait_sent(wo.at[0, 0], wo_send.at[0, 0])
        for slot in range(1, pairs):
            for lane in range(2):
                wait_sent(wo.at[0, 0, 0 : group // 2], wo_send.at[slot, lane])
            wait_sent(wo.at[0, 0], wo_send.at[slot, 2])

    def part_of(slot):
        return lax.rem(pair + slot, pairs)

    for slot in range(pairs):
        lane = lax.broadcasted_iota(jnp.int32, (quarter, span), 1)
        first = sp * count + part_of(slot) * span
        for n, table in enumerate(angle_tables(first + lane, quarter)):
            tabs[slot, n] = table
    for slot in range(1, pairs):
        for c in range(chunks):
            lane = lax.broadcasted_iota(jnp.int32, (quarter, 2 * sizes[c]), 1)
            lane = jnp.where(lane < sizes[c], lane, lane + (rows - sizes[c]))
            first = sp * count + part_of(slot) * span + starts[c]
            for n, table in enumerate(angle_tables(first + lane, quarter)):
                tabs_late[(slot - 1) * chunks + c][n] = table
    top[...] = jnp.full_like(top, -1e30)
    acc[...] = jnp.zeros_like(acc)
    pltpu.make_async_copy(wall, wall, local_sem.at[1]).wait()
    for load in loads[4:6]:
        load.wait()
    wall[:, query_cols:] = jnp.transpose(wkv[...])
    gains[...] = jnp.zeros_like(gains)
    gains[0:heads, 0:width] = qg[...].astype(F32) * (LOG2E * width ** (-0.5))
    gains[heads : heads + kv_heads, 0:width] = kg[...].astype(F32)
    turned_gains = jnp.transpose(gains[...])
    kv_rows = kv_heads * width

    def make_kv(x, tables, put):
        turned = jnp.transpose(x[:, 0:kv_rows])
        for g in range(kv_heads):
            gain = turned_gains[0:width, heads + g : heads + g + 1]
            keys = prepare(turned[g * width : (g + 1) * width], gain, tables)
            put(slice(g * width, (g + 1) * width), jnp.transpose(keys).astype(BF16))
        put(slice(kv_rows, 2 * kv_rows), x[:, kv_rows:].astype(BF16))

    def make_queries(slot):
        turned = jnp.transpose(raw[slot])
        tables = tuple(tabs[slot, n] for n in range(4))
        for g in range(kv_heads):
            made = []
            for h in range(g * share, (g + 1) * share):
                q = prepare(turned[h * width : (h + 1) * width], turned_gains[0:width, h : h + 1], tables)
                made.append(q.astype(BF16))
            queries[slot, g] = jnp.concatenate(made, axis=1)

    def kv_ref(unit):
        return kv_early if unit == 0 else kv_late[unit - 1]

    def kv_copy(unit, block, number, where):
        spot = kv_ref(unit).at[block]
        return send(spot, spot, kv_send.at[unit], kv_recv.at[unit, number], {"sp": where})

    def mirror(k):
        return cols + (0 if k < 2 else 1)

    def send_kv(unit):
        kv_copy(unit, sp, mirror(0), other).start()
        for k in range(1, cols):
            kv_copy(unit, sp, k, near_place(k) * 2 + side).start()

    def forward_kv(unit, start, stop):
        for k in range(start, stop):
            block = near_place(k) * 2 + side
            kv_copy(unit, block, k, other).wait_recv()
            kv_copy(unit, block, mirror(k), other).start()

    def mirrored_kv(unit, n):
        many = 2 if n == 0 else cols - 2
        wait_here(kv_ref(unit).at[0:many], kv_recv.at[unit, cols + n])

    def sent_kv(unit):
        wait_sent(kv_ref(unit).at[0 : n_sp - 1], kv_send.at[unit])

    loads[0].wait()
    wait_here(tok.at[0, 1 - core], tok_recv.at[0])
    depth = tok.shape[3]
    x = jnp.dot(tok[0].reshape(span, depth), wall[:, query_cols:], preferred_element_type=F32)

    def put_early(at, value):
        kv_early[sp, :, at] = value

    make_kv(x, tuple(tabs[0, n] for n in range(4)), put_early)
    send_kv(0)
    raw[0] = jnp.dot(tok[0].reshape(span, depth), wall[:, 0:query_cols], preferred_element_type=F32)
    make_queries(0)

    tiles = share * span // TILE

    def attend(loaders, slots):
        items = [(n, slot, g, t) for n in range(len(loaders)) for slot in slots for g in range(kv_heads) for t in range(tiles)]
        held = {}
        for n, load in enumerate(loaders):
            block = load()
            turned = jnp.transpose(block)
            ones = jnp.ones((ONES, block.shape[0]), BF16)
            for g in range(kv_heads):
                keys = block[:, g * width : (g + 1) * width]
                values = turned[kv_rows + g * width : kv_rows + (g + 1) * width]
                held[n, g] = (keys, jnp.concatenate([values, ones], axis=0))
        scores, weights = {}, {}

        def spot(i):
            _, slot, g, t = items[i]
            return (slot * kv_heads + g) * tiles + t

        def score(i):
            n, slot, g, t = items[i]
            q = queries[slot, g, :, t * TILE : (t + 1) * TILE]
            scores[i] = jnp.dot(held[n, g][0], q, preferred_element_type=F32)

        def soften(i):
            s = scores.pop(i)
            at = spot(i)
            old = top[at]
            new = jnp.maximum(old, jnp.max(s, axis=0, keepdims=True))
            top[at] = new
            weights[i] = (jnp.exp2(s - new).astype(BF16), jnp.exp2(old - new))

        def gather(i):
            n, slot, g, t = items[i]
            w, scale = weights.pop(i)
            at = spot(i)
            acc[at] = acc[at] * scale + jnp.dot(held[n, g][1], w, preferred_element_type=F32)

        total = len(items)
        for i in range(min(AHEAD, total)):
            score(i)
        for i in range(total):
            if i + AHEAD < total:
                score(i + AHEAD)
            if i >= BEHIND:
                gather(i - BEHIND)
            soften(i)
        for i in range(max(total - BEHIND, 0), total):
            gather(i)

    def early(k):
        place = near_place(k)
        return lambda: kv_early[pl.ds(pl.multiple_of(place * 2, 2), 2)].reshape(2 * span, 2 * kv_rows)

    def late_line(unit, k, way):
        def load():
            return jnp.concatenate([kv_late[unit - 1][(k + n) * 2 + way] for n in range(LINES)], axis=0)

        return load

    late_units = [1 + (slot - 1) * chunks + c for slot in range(1, pairs) for c in range(chunks)]
    late_order = [(slot, c) for c in range(chunks) for slot in range(1, pairs)]

    def token_first(slot, c):
        wait_here(tok.at[slot, core, rows_of(c)], tok_sem(0, slot, c))
        token_on(slot, c).start()

    def token_second(slot, c):
        unit = 1 + (slot - 1) * chunks + c
        wait_here(tok.at[slot, 1 - core, rows_of(c)], tok_sem(1, slot, c))
        piece = tok[slot, :, rows_of(c)].reshape(2 * sizes[c], depth)
        x = jnp.dot(piece, wall[:, query_cols:], preferred_element_type=F32)

        def put_late(at, value):
            kv_late[unit - 1][sp, :, at] = value

        make_kv(x, tuple(tabs_late[unit - 1][n] for n in range(4)), put_late)
        send_kv(unit)
        x = jnp.dot(piece, wall[:, 0:query_cols], preferred_element_type=F32)
        for which in range(2):
            at = slice(which * rows + starts[c], which * rows + starts[c] + sizes[c])
            raw[slot, at] = x[which * sizes[c] : (which + 1) * sizes[c]]

    def attend_early(slots, start, stop):
        for k in range(start, stop, LINES):
            attend([early(n) for n in range(k, min(k + LINES, stop))], slots)

    def attend_late(unit, way):
        for k in range(0, cols, LINES):
            attend([late_line(unit, k, way)], everyone)

    remote = list(range(1, pairs))
    everyone = remote + [0]
    firsts, last = late_units[:-1], late_units[-1]
    forward_kv(0, 1, 3)
    for slot, c in late_order[:1]:
        token_first(slot, c)
    forward_kv(0, 3, cols)
    for slot, c in late_order[:1]:
        token_second(slot, c)
    for slot, c in late_order[1:-1]:
        token_first(slot, c)
        token_second(slot, c)
    mirrored_kv(0, 0)
    attend_early([0], 0, 2)
    for slot, c in late_order[-1:]:
        token_first(slot, c)
        token_second(slot, c)
    for unit in firsts:
        forward_kv(unit, 1, cols)
    for slot in remote:
        make_queries(slot)
    mirrored_kv(0, 1)
    attend_early([0], 2, cols)
    forward_kv(last, 1, 2)
    wo_pass(0, 1)
    attend_early(remote, 0, 2)
    forward_kv(last, 2, 3)
    attend_early(remote, 2, cols)
    forward_kv(last, 3, cols)
    wo_pass(1, 3)
    for unit in firsts:
        attend_late(unit, side)
    wo_pass(3, 4)
    for unit in firsts:
        mirrored_kv(unit, 0)
        mirrored_kv(unit, 1)
        attend_late(unit, 1 - side)
    wo_pass(4, 5)
    attend_late(last, side)
    wo_pass(5, 6)
    mirrored_kv(last, 0)
    mirrored_kv(last, 1)
    attend_late(last, 1 - side)
    wo_pass(6, 7)

    logs = {}

    def att_copy(slot, which):
        there = 0 if slot == 0 else pairs - slot
        return send(
            att_out.at[slot, which],
            att_in.at[there, core],
            att_send.at[slot],
            att_recv.at[there],
            {"tp": part_of(slot) * 2 + which},
        )

    for slot in everyone:
        turned = []
        for g in range(kv_heads):
            made, sums = [], []
            for t in range(tiles):
                at = (slot * kv_heads + g) * tiles + t
                total = acc[at, width : width + 1, :]
                made.append((acc[at, 0:width, :] * (1.0 / total)).astype(BF16))
                sums.append((top[at] + jnp.log2(total)) * LN2)
            turned.append(jnp.transpose(jnp.concatenate(made, axis=1)))
            logs[slot, g] = jnp.concatenate(sums, axis=1)
        for which in range(2):
            piece = jnp.concatenate(
                [
                    turned[g][h * span + which * rows : h * span + (which + 1) * rows]
                    for g in range(kv_heads)
                    for h in range(share)
                ],
                axis=1,
            )
            if slot:
                att_out[slot, which] = piece
                att_copy(slot, which).start()
            else:

                @pl.when(core == which)
                def _():
                    att_in[0, which] = piece

                @pl.when(core != which)
                def _():
                    att_out[0, which] = piece

    att_copy(0, 1 - core).start()
    wo_pass(7, 8)
    for g in range(kv_heads):
        for h in range(share):
            lines = [logs[slot, g][:, h * span : (h + 1) * span] for slot in range(pairs)]
            for part in range(pairs):
                line = lines[0]
                for slot in range(1, pairs):
                    line = jnp.where(part_of(slot) == part, lines[slot], line)
                log_ref[g * share + h : g * share + h + 1, part * span : (part + 1) * span] = line

    wo_take(0, 4)
    loads[6].wait()
    wait_here(wo.at[0, 1 - core], wo_recv.at[0, 0])

    model = wo.shape[3]
    step_cols = 512
    wait_here(att_in.at[0, 1 - core], att_recv.at[0])
    for n in range(model // step_cols):
        at = slice(n * step_cols, (n + 1) * step_cols)
        res[:, at] = jnp.dot(att_in[0, 0], wo[0, 0, :, at], preferred_element_type=F32) + jnp.dot(
            att_in[0, 1], wo[0, 1, :, at], preferred_element_type=F32
        )
    wo_take(4, 8)
    for unit in [0] + late_units:
        sent_kv(unit)
    tokens_sent()
    for slot in range(1, pairs):
        wait_here(att_in.at[slot], att_recv.at[slot])
    wo_last()
    for n in range(model // step_cols):
        at = slice(n * step_cols, (n + 1) * step_cols)
        total = res[:, at]
        for slot in range(1, pairs):
            for which in range(2):
                total = total + jnp.dot(att_in[slot, which], wo[slot, which, :, at], preferred_element_type=F32)
        mixed_ref[:, at] = total.astype(BF16)

    wait_sent(att_out.at[0, 0], att_send.at[0])
    for slot in range(1, pairs):
        wait_sent(att_out.at[slot], att_send.at[slot])
    wo_sent()


def body(n_sp, n_tp, tokens, query_weight, key_weight, value_weight, out_weight, query_gain, key_gain):
    rows, depth = tokens.shape
    query_cols = query_weight.shape[1]
    kv_cols = key_weight.shape[1]
    heads, width = query_gain.shape
    kv_heads = key_gain.shape[0]
    group, model = out_weight.shape
    count = rows * n_tp
    pairs, cols = n_tp // 2, n_sp // 2
    sizes = (rows * 2 // 3, rows - rows * 2 // 3)
    chunks = len(sizes)
    span = 2 * rows
    units = 1 + (pairs - 1) * chunks
    spots = pairs * heads * span // TILE
    any_space = pl.BlockSpec(memory_space=pl.ANY)
    vmem = pl.BlockSpec(memory_space=pltpu.VMEM)
    dma = pltpu.SemaphoreType.DMA
    return pl.pallas_call(
        functools.partial(kernel, n_sp, n_tp, sizes),
        out_shape=(
            pltpu.VMEM((rows, model), BF16),
            pltpu.VMEM((heads, count), F32),
        ),
        in_specs=[any_space] * 7,
        out_specs=(vmem, vmem),
        scratch_shapes=[
            pltpu.VMEM((pairs, 2, rows, depth), BF16),
            pltpu.VMEM((depth, query_cols + 2 * kv_cols), BF16),
            pltpu.VMEM((2 * kv_cols, depth), BF16),
            pltpu.VMEM((pairs, 2, group, model), BF16),
            pltpu.VMEM((heads, width), BF16),
            pltpu.VMEM((kv_heads, width), BF16),
            pltpu.VMEM((128, 128), F32),
            pltpu.VMEM((pairs, span, query_cols), F32),
            pltpu.VMEM((pairs, 4, width // 4, span), F32),
            [pltpu.VMEM((4, width // 4, 2 * size), F32) for size in sizes] * (pairs - 1),
            pltpu.VMEM((pairs, kv_heads, width, heads // kv_heads * span), BF16),
            pltpu.VMEM((n_sp, span, 2 * kv_cols), BF16),
            [pltpu.VMEM((n_sp, 2 * size, 2 * kv_cols), BF16) for size in sizes] * (pairs - 1),
            pltpu.VMEM((spots, 1, TILE), F32),
            pltpu.VMEM((spots, width + ONES, TILE), F32),
            pltpu.VMEM((pairs, 2, rows, group), BF16),
            pltpu.VMEM((pairs, 2, rows, group), BF16),
            pltpu.VMEM((rows, model), F32),
            dma((5,)),
            dma((2 * pairs,)),
            dma((2 * pairs * chunks,)),
            dma((pairs, 3)),
            dma((pairs, 4 * SUBS + 1)),
            dma((units,)),
            dma((units, cols + 2)),
            dma((pairs,)),
            dma((pairs,)),
        ],
        compiler_params=pltpu.CompilerParams(
            collective_id=0, has_side_effects=True, vmem_limit_bytes=60 * 1024 * 1024
        ),
        name="attention",
    )(tokens, query_weight, key_weight.T, value_weight.T, out_weight, query_gain, key_gain)


def solution(mesh):
    return jax.shard_map(
        functools.partial(body, mesh.shape["sp"], mesh.shape["tp"]),
        mesh=mesh,
        in_specs=(
            P(("sp", "tp"), None),
            P(None, "tp"),
            P(None, "tp"),
            P(None, "tp"),
            P("tp", None),
            P("tp", None),
            P("tp", None),
        ),
        out_specs=(P(("sp", "tp"), None), P("tp", "sp")),
        check_vma=False,
    )
```

time: 46.7 us -> 34.8 us (0.75)
  Pallas kernels: 44.5 us -> 32.3 us
    pallas_call x1, Pallas kernels: 44.5 us -> 32.3 us  [body(): pl.pallas_call(functools.partial(kernel, n_sp, n_tp, sizes), out_shape=(p...]
where the time goes in v1:
time: 34.8 us; the launch traced here: 34.3 us
  Pallas kernels  32.3 us (93%)
  local copies, waits for them, and re-layouts  1.34 us (4%)
  between operations  0.64 us (2%)
    pallas_call x1, Pallas kernels, body(): pl.pallas_call(functools.partial(kernel, n_sp, n_tp, sizes), out_shape=(p...  32.3 us
    unnamed x2, local copies, waits for them, and re-layouts  1.34 us

profile of v1, /device:TPU:0, one launch (start us, length us, event | category | flops | bytes accessed | tf_op | source)
XLA Modules:
  0.0 34.3 jit_solution(18390289652035381589)
XLA Ops:
  0.6 32.3 %attention.1 = (bf16[96,2048]{1,0:T(8,128)(2,1)S(1)}, f32[4,384]{1,0:T(4,128)S(1)}) custom-call(bf16[96,2048]{1,0:T(8,128)(2,1)} %tok_hbm.1, bf16[2048,256]{1,0:T(8,128)(2,1)} %wq_hbm.1, bf16[64,2048]{1,0:T(8,128)(2,1)} %bitcast.2, bf16[64,2048]{1,0:T(8,128)(2,1)} %bitcast.3, bf16[256,2048]{1,0:T(8,128)(2,1)} %wo_hbm.1, bf16[4,64]{1,0:T(4,128)(2,1)} %qg_hbm.1, ...), custom_call_target="tpu_custom_call" | custom-call | tf_op jit(solution)/shard_map/attention/pallas_call | solution.py:585
  33.0 0.7 %copy.11 = bf16[96,2048]{1,0:T(8,128)(2,1)} copy(bf16[96,2048]{1,0:T(8,128)(2,1)S(1)} %get-tuple-element.2) | data formatting | bytes 786432
  33.7 0.6 %copy.12 = f32[4,384]{1,0:T(4,128)} copy(f32[4,384]{1,0:T(4,128)S(1)} %get-tuple-element.3) | data formatting | bytes 12288

commit v2 on v1

--- a/solution.py
+++ b/solution.py
@@ -18,7 +18,9 @@
 AHEAD = 3
 BEHIND = 3
 LINES = 4
-SUBS = 4
+UNITS = 16
+ACROSS = 6
+ASIDE = 5
 MESH = pl.DeviceIdType.MESH
 F32 = jnp.float32
 BF16 = jnp.bfloat16
@@ -172,87 +174,110 @@
         return slice(starts[c], starts[c] + sizes[c])
 
     def tok_sem(which, slot, c):
-        return tok_recv.at[(slot * 2 + which) * chunks + c]
+        return tok_recv.at[1 + ((slot - 1) * 2 + which) * chunks + c]
 
     def token_over(i, c):
         slot = pairs - i
         return send(
-            tok_hbm.at[rows_of(c)],
+            tok.at[0, core, rows_of(c)],
             tok.at[slot, core, rows_of(c)],
-            tok_send.at[2 * i],
+            tok_send.at[2 * i - 1],
             tok_sem(0, slot, c),
             {"tp": across(i)},
         )
 
     def token_on(slot, c):
         spot = tok.at[slot, core, rows_of(c)]
-        return send(spot, spot, tok_send.at[2 * slot + 1], tok_sem(1, slot, c), {"tp": mate})
-
+        return send(spot, spot, tok_send.at[2 * slot], tok_sem(1, slot, c), {"tp": mate})
+
+    loads[0].wait()
     for c in range(chunks):
         for i in range(1, pairs):
             token_over(i, c).start()
-    send(tok_hbm, tok.at[0, core], tok_send.at[0], tok_recv.at[0], {"tp": mate}).start()
+    send(tok.at[0, core], tok.at[0, core], tok_send.at[0], tok_recv.at[0], {"tp": mate}).start()
 
     def tokens_sent():
-        for n in range(2 * pairs):
-            if n != 1:
-                wait_sent(tok.at[0, 0], tok_send.at[n])
-
-    sub_rows = group // (4 * SUBS)
-    shares = [(way, h) for h in range(SUBS) for way in (1, 0)]
+        for n in range(2 * pairs - 1):
+            wait_sent(tok.at[0, 0], tok_send.at[n])
+
+    unit_rows = group // UNITS
+    color = sp % 4
+    colors = (color + 1 - 2 * (color % 2), (color + 2) % 4)
+    color_far = 3 - color
     sides = (side, col % 2)
     friends = (other, beside)
 
-    def wo_rows(way, whose, h):
-        at = (2 * way + whose) * SUBS + h
-        return pl.ds(pl.multiple_of(at * sub_rows, sub_rows), sub_rows)
-
-    def wo_sem(slot, own, way, h):
-        return wo_recv.at[slot, (own * 2 + way) * SUBS + h]
-
-    def wo_over(i, way, h):
+    def ring_unit(whose, h):
+        return whose * 2 + h
+
+    def swap_unit(way, whose, h):
+        return 8 + way * 4 + whose * 2 + h
+
+    def wo_at(ref, unit):
+        return ref.at[pl.ds(pl.multiple_of(unit * unit_rows, unit_rows), unit_rows)]
+
+    def arrival(slot, number):
+        return 1 + (slot - 1) * (ACROSS + 2 * ASIDE + 1) + number
+
+    over = [(ring_unit(color, h), h) for h in range(2)]
+    over += [(swap_unit(way, sides[way], h), 2 + way * 2 + h) for h in range(2) for way in (1, 0)]
+
+    def wo_over(i, unit, number):
         slot = pairs - i
-        at = wo_rows(way, sides[way], h)
         return send(
-            wo_hbm.at[at], wo.at[slot, core, at], wo_send.at[i, 0], wo_sem(slot, 0, way, h), {"tp": across(i)}
+            wo_at(wo_hbm, unit), wo_at(wo.at[slot, core], unit), wo_send.at[3 * i - 2 + 0], wo_recv.at[arrival(slot, number)], {"tp": across(i)}
         )
 
-    def wo_on(slot, way, h):
-        spot = wo.at[slot, core, wo_rows(way, sides[way], h)]
-        return send(spot, spot, wo_send.at[slot, 1], wo_sem(slot, 1, way, h), {"sp": friends[way]})
-
-    def wo_give(slot, way, whose, h):
-        spot = wo.at[slot, core, wo_rows(way, whose, h)]
-        return send(spot, spot, wo_send.at[slot, 2], wo_recv.at[slot, 4 * SUBS], {"tp": mate})
-
-    send(wo_hbm, wo.at[0, core], wo_send.at[0, 0], wo_recv.at[0, 0], {"tp": mate}).start()
-    for way, h in shares:
+    def wo_aside(slot, unit, way, number):
+        spot = wo_at(wo.at[slot, core], unit)
+        return send(spot, spot, wo_send.at[3 * slot - 2 + 1], wo_recv.at[arrival(slot, ACROSS + way * ASIDE + number)], {"sp": friends[way]})
+
+    def wo_got(slot, unit, number):
+        spot = wo_at(wo.at[slot, core], unit)
+        wait_here(spot, wo_recv.at[arrival(slot, number)])
+        send(spot, spot, wo_send.at[3 * slot - 2 + 2], wo_recv.at[arrival(slot, ACROSS + 2 * ASIDE)], {"tp": mate}).start()
+
+    send(wo_hbm, wo.at[0, core], wo_send.at[0], wo_recv.at[0], {"tp": mate}).start()
+    for unit, number in over:
         for i in range(1, pairs):
-            wo_over(i, way, h).start()
-
-    def wo_pass(start, stop):
-        for way, h in shares[start:stop]:
-            for slot in range(1, pairs):
-                wait_here(wo.at[slot, core, wo_rows(way, sides[way], h)], wo_sem(slot, 0, way, h))
-                wo_on(slot, way, h).start()
-                wo_give(slot, way, sides[way], h).start()
-
-    def wo_take(start, stop):
-        for way, h in shares[start:stop]:
-            for slot in range(1, pairs):
-                wait_here(wo.at[slot, core, wo_rows(way, 1 - sides[way], h)], wo_sem(slot, 1, way, h))
-                wo_give(slot, way, 1 - sides[way], h).start()
+            wo_over(i, unit, number).start()
+
+    def ring_first(h):
+        for slot in range(1, pairs):
+            wo_got(slot, ring_unit(color, h), h)
+            for way in range(2):
+                wo_aside(slot, ring_unit(color, h), way, h).start()
+
+    def ring_second(h):
+        for slot in range(1, pairs):
+            for way in range(2):
+                wo_got(slot, ring_unit(colors[way], h), ACROSS + way * ASIDE + h)
+                if way != h:
+                    wo_aside(slot, ring_unit(colors[way], h), 1 - way, 4).start()
+
+    def ring_third(h):
+        for slot in range(1, pairs):
+            wo_got(slot, ring_unit(color_far, h), ACROSS + h * ASIDE + 4)
+
+    def swap_first(way, h):
+        for slot in range(1, pairs):
+            wo_got(slot, swap_unit(way, sides[way], h), 2 + way * 2 + h)
+            wo_aside(slot, swap_unit(way, sides[way], h), way, 2 + h).start()
+
+    def swap_second(way, h):
+        for slot in range(1, pairs):
+            wo_got(slot, swap_unit(way, 1 - sides[way], h), ACROSS + way * ASIDE + 2 + h)
 
     def wo_last():
         for slot in range(1, pairs):
-            wait_here(wo.at[slot, 1 - core], wo_recv.at[slot, 4 * SUBS])
+            wait_here(wo.at[slot, 1 - core], wo_recv.at[arrival(slot, ACROSS + 2 * ASIDE)])
 
     def wo_sent():
-        wait_sent(wo.at[0, 0], wo_send.at[0, 0])
-        for slot in range(1, pairs):
-            for lane in range(2):
-                wait_sent(wo.at[0, 0, 0 : group // 2], wo_send.at[slot, lane])
-            wait_sent(wo.at[0, 0], wo_send.at[slot, 2])
+        wait_sent(wo.at[0, 0], wo_send.at[0])
+        for slot in range(1, pairs):
+            wait_sent(wo.at[0, 0, 0 : ACROSS * unit_rows], wo_send.at[3 * slot - 2 + 0])
+            wait_sent(wo.at[0, 0, 0 : 2 * ASIDE * unit_rows], wo_send.at[3 * slot - 2 + 1])
+            wait_sent(wo.at[0, 0], wo_send.at[3 * slot - 2 + 2])
 
     def part_of(slot):
         return lax.rem(pair + slot, pairs)
@@ -306,11 +331,8 @@
         spot = kv_ref(unit).at[block]
         return send(spot, spot, kv_send.at[unit], kv_recv.at[unit, number], {"sp": where})
 
-    def mirror(k):
-        return cols + (0 if k < 2 else 1)
-
     def send_kv(unit):
-        kv_copy(unit, sp, mirror(0), other).start()
+        kv_copy(unit, sp, 0 if unit else cols, other).start()
         for k in range(1, cols):
             kv_copy(unit, sp, k, near_place(k) * 2 + side).start()
 
@@ -318,16 +340,17 @@
         for k in range(start, stop):
             block = near_place(k) * 2 + side
             kv_copy(unit, block, k, other).wait_recv()
-            kv_copy(unit, block, mirror(k), other).start()
-
-    def mirrored_kv(unit, n):
-        many = 2 if n == 0 else cols - 2
-        wait_here(kv_ref(unit).at[0:many], kv_recv.at[unit, cols + n])
+            kv_copy(unit, block, 0, other).start()
+
+    def mirrored_kv(unit):
+        if unit == 0:
+            wait_here(kv_early.at[0 : cols - 1], kv_recv.at[0, 0])
+        else:
+            wait_here(kv_ref(unit).at[0:cols], kv_recv.at[unit, 0])
 
     def sent_kv(unit):
         wait_sent(kv_ref(unit).at[0 : n_sp - 1], kv_send.at[unit])
 
-    loads[0].wait()
     wait_here(tok.at[0, 1 - core], tok_recv.at[0])
     depth = tok.shape[3]
     x = jnp.dot(tok[0].reshape(span, depth), wall[:, query_cols:], preferred_element_type=F32)
@@ -390,9 +413,11 @@
         for i in range(max(total - BEHIND, 0), total):
             gather(i)
 
-    def early(k):
-        place = near_place(k)
-        return lambda: kv_early[pl.ds(pl.multiple_of(place * 2, 2), 2)].reshape(2 * span, 2 * kv_rows)
+    def early_blocks(*blocks):
+        def load():
+            return jnp.concatenate([kv_early[near_place(k) * 2 + way] for k, way in blocks], axis=0)
+
+        return load
 
     def late_line(unit, k, way):
         def load():
@@ -423,17 +448,19 @@
             at = slice(which * rows + starts[c], which * rows + starts[c] + sizes[c])
             raw[slot, at] = x[which * sizes[c] : (which + 1) * sizes[c]]
 
-    def attend_early(slots, start, stop):
-        for k in range(start, stop, LINES):
-            attend([early(n) for n in range(k, min(k + LINES, stop))], slots)
-
-    def attend_late(unit, way):
+    def attend_early(slots, ways):
         for k in range(0, cols, LINES):
-            attend([late_line(unit, k, way)], everyone)
+            attend([early_blocks((k + n, way), (k + n + 1, way)) for way in ways for n in range(0, LINES, 2)], slots)
+
+    def attend_late(units, ways, slots):
+        for k in range(0, cols, LINES):
+            attend([late_line(unit, k, way) for unit in units for way in ways], slots)
 
     remote = list(range(1, pairs))
     everyone = remote + [0]
     firsts, last = late_units[:-1], late_units[-1]
+    wait_here(kv_early.at[0], kv_recv.at[0, cols])
+    attend([early_blocks((0, side), (0, 1 - side))], [0])
     forward_kv(0, 1, 3)
     for slot, c in late_order[:1]:
         token_first(slot, c)
@@ -443,38 +470,40 @@
     for slot, c in late_order[1:-1]:
         token_first(slot, c)
         token_second(slot, c)
-    mirrored_kv(0, 0)
-    attend_early([0], 0, 2)
+    attend([early_blocks(*((n, side) for n in range(1, LINES)))], [0])
     for slot, c in late_order[-1:]:
         token_first(slot, c)
+    for unit in firsts:
+        forward_kv(unit, 1, 2)
+    for slot, c in late_order[-1:]:
         token_second(slot, c)
     for unit in firsts:
-        forward_kv(unit, 1, cols)
+        forward_kv(unit, 2, cols)
+    ring_first(0)
     for slot in remote:
         make_queries(slot)
-    mirrored_kv(0, 1)
-    attend_early([0], 2, cols)
+    mirrored_kv(0)
+    attend([early_blocks(*((n, 1 - side) for n in range(1, LINES)))], [0])
+    for k in range(LINES, cols, LINES):
+        attend([early_blocks((k + n, way), (k + n + 1, way)) for way in (side, 1 - side) for n in range(0, LINES, 2)], [0])
+    ring_first(1)
     forward_kv(last, 1, 2)
-    wo_pass(0, 1)
-    attend_early(remote, 0, 2)
-    forward_kv(last, 2, 3)
-    attend_early(remote, 2, cols)
-    forward_kv(last, 3, cols)
-    wo_pass(1, 3)
+    swap_first(1, 0)
+    attend_early(remote, [side])
+    forward_kv(last, 2, cols)
+    attend_early(remote, [1 - side])
+    swap_first(0, 0)
     for unit in firsts:
-        attend_late(unit, side)
-    wo_pass(3, 4)
-    for unit in firsts:
-        mirrored_kv(unit, 0)
-        mirrored_kv(unit, 1)
-        attend_late(unit, 1 - side)
-    wo_pass(4, 5)
-    attend_late(last, side)
-    wo_pass(5, 6)
-    mirrored_kv(last, 0)
-    mirrored_kv(last, 1)
-    attend_late(last, 1 - side)
-    wo_pass(6, 7)
+        mirrored_kv(unit)
+    attend_late(firsts, [side, 1 - side], remote)
+    swap_first(1, 1)
+    ring_second(0)
+    attend_late(firsts, [side, 1 - side], [0])
+    swap_first(0, 1)
+    ring_second(1)
+    swap_second(1, 0)
+    mirrored_kv(last)
+    attend_late([last], [side, 1 - side], remote)
 
     logs = {}
 
@@ -488,7 +517,7 @@
             {"tp": part_of(slot) * 2 + which},
         )
 
-    for slot in everyone:
+    def finish(slot):
         turned = []
         for g in range(kv_heads):
             made, sums = [], []
@@ -521,8 +550,13 @@
                 def _():
                     att_out[0, which] = piece
 
+    for slot in remote:
+        finish(slot)
+    attend_late([last], [side, 1 - side], [0])
+    finish(0)
     att_copy(0, 1 - core).start()
-    wo_pass(7, 8)
+    swap_second(0, 0)
+    ring_third(0)
     for g in range(kv_heads):
         for h in range(share):
             lines = [logs[slot, g][:, h * span : (h + 1) * span] for slot in range(pairs)]
@@ -532,9 +566,8 @@
                     line = jnp.where(part_of(slot) == part, lines[slot], line)
                 log_ref[g * share + h : g * share + h + 1, part * span : (part + 1) * span] = line
 
-    wo_take(0, 4)
     loads[6].wait()
-    wait_here(wo.at[0, 1 - core], wo_recv.at[0, 0])
+    wait_here(wo.at[0, 1 - core], wo_recv.at[0])
 
     model = wo.shape[3]
     step_cols = 512
@@ -544,19 +577,24 @@
         res[:, at] = jnp.dot(att_in[0, 0], wo[0, 0, :, at], preferred_element_type=F32) + jnp.dot(
             att_in[0, 1], wo[0, 1, :, at], preferred_element_type=F32
         )
-    wo_take(4, 8)
+    swap_second(1, 1)
+    ring_third(1)
+    swap_second(0, 1)
     for unit in [0] + late_units:
         sent_kv(unit)
     tokens_sent()
     for slot in range(1, pairs):
         wait_here(att_in.at[slot], att_recv.at[slot])
+    for slot in range(1, pairs):
+        for n in range(model // step_cols):
+            at = slice(n * step_cols, (n + 1) * step_cols)
+            res[:, at] += jnp.dot(att_in[slot, core], wo[slot, core, :, at], preferred_element_type=F32)
     wo_last()
     for n in range(model // step_cols):
         at = slice(n * step_cols, (n + 1) * step_cols)
         total = res[:, at]
         for slot in range(1, pairs):
-            for which in range(2):
-                total = total + jnp.dot(att_in[slot, which], wo[slot, which, :, at], preferred_element_type=F32)
+            total = total + jnp.dot(att_in[slot, 1 - core], wo[slot, 1 - core, :, at], preferred_element_type=F32)
         mixed_ref[:, at] = total.astype(BF16)
 
     wait_sent(att_out.at[0, 0], att_send.at[0])
@@ -574,7 +612,7 @@
     group, model = out_weight.shape
     count = rows * n_tp
     pairs, cols = n_tp // 2, n_sp // 2
-    sizes = (rows * 2 // 3, rows - rows * 2 // 3)
+    sizes = (rows // 2, rows - rows // 2)
     chunks = len(sizes)
     span = 2 * rows
     units = 1 + (pairs - 1) * chunks
@@ -610,12 +648,12 @@
             pltpu.VMEM((pairs, 2, rows, group), BF16),
             pltpu.VMEM((rows, model), F32),
             dma((5,)),
-            dma((2 * pairs,)),
-            dma((2 * pairs * chunks,)),
-            dma((pairs, 3)),
-            dma((pairs, 4 * SUBS + 1)),
+            dma((2 * pairs - 1,)),
+            dma((1 + (pairs - 1) * 2 * chunks,)),
+            dma((1 + (pairs - 1) * 3,)),
+            dma((1 + (pairs - 1) * (ACROSS + 2 * ASIDE + 1),)),
             dma((units,)),
-            dma((units, cols + 2)),
+            dma((units, cols + 1)),
             dma((pairs,)),
             dma((pairs,)),
         ],

time: 34.8 us -> 34.2 us (0.983)
  no operation moved by 1% of the time
where the time goes in v2:
time: 34.2 us; the launch traced here: 34 us
  Pallas kernels  32 us (94%)
  local copies, waits for them, and re-layouts  1.34 us (4%)
  between operations  0.64 us (2%)
    pallas_call x1, Pallas kernels, body(): pl.pallas_call(functools.partial(kernel, n_sp, n_tp, sizes), out_shape=(p...  32 us
    unnamed x2, local copies, waits for them, and re-layouts  1.34 us

profile of v2, /device:TPU:0, one launch (start us, length us, event | category | flops | bytes accessed | tf_op | source)
XLA Modules:
  0.0 34.0 jit_solution(10746659838515195604)
XLA Ops:
  0.6 32.0 %attention.1 = (bf16[96,2048]{1,0:T(8,128)(2,1)S(1)}, f32[4,384]{1,0:T(4,128)S(1)}) custom-call(bf16[96,2048]{1,0:T(8,128)(2,1)} %tok_hbm.1, bf16[2048,256]{1,0:T(8,128)(2,1)} %wq_hbm.1, bf16[64,2048]{1,0:T(8,128)(2,1)} %bitcast.2, bf16[64,2048]{1,0:T(8,128)(2,1)} %bitcast.3, bf16[256,2048]{1,0:T(8,128)(2,1)} %wo_hbm.1, bf16[4,64]{1,0:T(4,128)(2,1)} %qg_hbm.1, ...), custom_call_target="tpu_custom_call" | custom-call | tf_op jit(solution)/shard_map/attention/pallas_call | solution.py:623
  32.7 0.7 %copy.11 = bf16[96,2048]{1,0:T(8,128)(2,1)} copy(bf16[96,2048]{1,0:T(8,128)(2,1)S(1)} %get-tuple-element.2) | data formatting | bytes 786432
  33.4 0.6 %copy.12 = f32[4,384]{1,0:T(4,128)} copy(f32[4,384]{1,0:T(4,128)S(1)} %get-tuple-element.3) | data formatting | bytes 12288

commit v3 on v2

--- a/solution.py
+++ b/solution.py
@@ -486,8 +486,8 @@
     attend([early_blocks(*((n, 1 - side) for n in range(1, LINES)))], [0])
     for k in range(LINES, cols, LINES):
         attend([early_blocks((k + n, way), (k + n + 1, way)) for way in (side, 1 - side) for n in range(0, LINES, 2)], [0])
+    forward_kv(last, 1, 2)
     ring_first(1)
-    forward_kv(last, 1, 2)
     swap_first(1, 0)
     attend_early(remote, [side])
     forward_kv(last, 2, cols)

time: 34.2 us -> 34.2 us (level)
  no operation moved by 1% of the time
where the time goes in v3:
time: 34.2 us; the launch traced here: 34.1 us
  Pallas kernels  32.1 us (94%)
  local copies, waits for them, and re-layouts  1.34 us (4%)
  between operations  0.64 us (2%)
    pallas_call x1, Pallas kernels, body(): pl.pallas_call(functools.partial(kernel, n_sp, n_tp, sizes), out_shape=(p...  32.1 us
    unnamed x2, local copies, waits for them, and re-layouts  1.34 us

profile of v3, /device:TPU:0, one launch (start us, length us, event | category | flops | bytes accessed | tf_op | source)
XLA Modules:
  0.0 34.1 jit_solution(9793138836242224453)
XLA Ops:
  0.6 32.1 %attention.1 = (bf16[96,2048]{1,0:T(8,128)(2,1)S(1)}, f32[4,384]{1,0:T(4,128)S(1)}) custom-call(bf16[96,2048]{1,0:T(8,128)(2,1)} %tok_hbm.1, bf16[2048,256]{1,0:T(8,128)(2,1)} %wq_hbm.1, bf16[64,2048]{1,0:T(8,128)(2,1)} %bitcast.2, bf16[64,2048]{1,0:T(8,128)(2,1)} %bitcast.3, bf16[256,2048]{1,0:T(8,128)(2,1)} %wo_hbm.1, bf16[4,64]{1,0:T(4,128)(2,1)} %qg_hbm.1, ...), custom_call_target="tpu_custom_call" | custom-call | tf_op jit(solution)/shard_map/attention/pallas_call | solution.py:623
  32.7 0.7 %copy.11 = bf16[96,2048]{1,0:T(8,128)(2,1)} copy(bf16[96,2048]{1,0:T(8,128)(2,1)S(1)} %get-tuple-element.2) | data formatting | bytes 786432
  33.5 0.6 %copy.12 = f32[4,384]{1,0:T(4,128)} copy(f32[4,384]{1,0:T(4,128)S(1)} %get-tuple-element.3) | data formatting | bytes 12288
